TPU v7x, 32 devices: a whole 2x2x4 slice. The times are simulated.
32 devices in a mesh: gr: 2 (over x), sp: 8 (over z, y), tp: 2 (over core).
Axes of the slice: x: 2, y: 2, z: 4, core: 2. Of those that a mesh axis runs over, the one named last changes fastest.
Arguments:
- tokens: bfloat16 [8, 2048, 2048], P('gr', 'sp'), parts along dimension 0, may hold values from -6 to 6
- new_rows: bfloat16 [8, 2048], P('gr'), parts along dimension 0, may hold values from -6 to 6
- new_query: bfloat16 [8, 1024], P('gr', 'tp'), parts along dimension 0, may hold values from -6 to 6
- norm_gain: bfloat16 [2048], replicated, may hold values from 0.099609375 to 1.8984375
- key_weight: bfloat16 [2048, 1024], P('sp', 'tp'), may hold values from -0.125 to 0.125
- value_weight: bfloat16 [2048, 2048], P('sp', 'tp'), may hold values from -0.125 to 0.125
- input_weight: bfloat16 [2048, 16], replicated, may hold values from -0.125 to 0.125
- forget_weight: bfloat16 [2048, 16], replicated, may hold values from -0.125 to 0.125
- forget_bias: float32 [16], P('tp'), may hold values from 3 to 12
- gate_offsets: float32 [8, 2048, 2, 16], P('gr', 'sp', None, 'tp'), parts along dimension 0, may hold values from -6 to 250, as said below
Outputs:
- cache_keys: bfloat16 [16, 1024, 1024], P(('gr', 'sp'), None, 'tp'), parts along dimension 0
- cache_values: bfloat16 [16, 1024, 2048], P(('gr', 'sp'), None, 'tp'), parts along dimension 0
- cache_weights: float32 [16, 16, 1024], P(('gr', 'sp'), 'tp'), parts along dimension 0
- first_read: bfloat16 [8, 2048], P('gr', 'tp'), parts along dimension 0
There are 2 independent parts, one for each index of `gr`. A program takes and returns all parts, laid end to end along the dimension named above; an argument that names none is the same for every part. Nothing has to cross between parts.
Inputs may be any that keep to these rules, and one draw needn't show every extreme that they name: `gate_offsets`: entry 1 along the third dimension is never positive.
All inputs are finite; a program needn't handle non-finite values.
Results may differ from a plain program's by a relative error of at most 0.012.
The roundings to bfloat16 on the way count: a program that leaves them out, or rounds other values in their place, can miss the bound.
Values may be sent and summed in bfloat16 or wider, within the bound.
A program may use at most 64 MiB of HBM per device.

v0:
```python
import jax
import jax.numpy as jnp
from jax import lax
from jax.sharding import PartitionSpec as P

EPSILON = 1e-06
HIGHEST = lax.Precision.HIGHEST


def normed_rows(source, norm_gain):
    widened = source.astype(jnp.float32)
    inverse_rms = lax.rsqrt(jnp.mean(widened * widened, axis=-1, keepdims=True) + EPSILON)
    return (widened * inverse_rms * norm_gain.astype(jnp.float32)).astype(jnp.bfloat16)


def contract_last(a, b):
    return lax.dot_general(a, b, (((1,), (1,)), ((), ())), preferred_element_type=jnp.float32)


def log_weights(gates, offsets, forget_bias, heads, blocks, pieces):
    rows = gates.shape[1]
    sub = rows // blocks
    input_gate = gates[:heads] + offsets[:heads]
    log_forget = jax.nn.log_sigmoid(gates[heads:] + forget_bias[:, None]) + offsets[heads:]
    by_block = log_forget.reshape(heads, blocks, sub)
    later = jnp.tril(jnp.ones((sub, sub), jnp.float32), -1)
    within = jnp.dot(by_block.reshape(heads * blocks, sub), later, precision=HIGHEST)
    totals = jnp.sum(by_block, axis=2)
    index = lax.axis_index("sp")
    everything = lax.all_gather(totals, "sp")
    ours = lax.dynamic_slice_in_dim(everything, index // pieces * pieces, pieces, 0)
    piece = index % pieces
    all_pieces = jnp.sum(ours, axis=0)
    after = jnp.flip(jnp.cumsum(jnp.flip(all_pieces, 1), axis=1), 1) - all_pieces
    follows = (jnp.arange(pieces) > piece).astype(jnp.float32)
    after = after + jnp.sum(ours * follows[:, None, None], axis=0)
    suffix = within.reshape(heads, blocks, sub) + after[:, :, None]
    return input_gate + suffix.reshape(heads, rows)


def read_part(query, keys, values, log_weight, heads):
    key_size = keys.shape[1] // heads
    value_size = values.shape[1] // heads
    peak = jnp.max(log_weight, axis=1, keepdims=True)
    own_head = jnp.arange(heads)[:, None] == jnp.arange(keys.shape[1])[None, :] // key_size
    spread = jnp.where(own_head, query, jnp.zeros_like(query))
    scores = contract_last(spread, keys)
    terms = jnp.exp(log_weight - peak) * scores
    wide = jnp.dot(terms.astype(jnp.bfloat16), values, preferred_element_type=jnp.float32)
    pick = jnp.eye(heads, dtype=jnp.float32)
    numerator = jnp.sum(wide.reshape(heads, heads, value_size) * pick[:, :, None], axis=1)
    return (peak, numerator, jnp.sum(terms, axis=1, keepdims=True))


def finish(peak, numerator, denominator, own_score, gate_new, value_new, seq_count, pieces):
    heads, value_size = numerator.shape
    one = jnp.concatenate([peak, denominator, own_score, gate_new], axis=1)
    one = jnp.pad(one, ((0, 0), (0, value_size - one.shape[1])))
    packed = jnp.concatenate([numerator, value_new, one], axis=1)
    everything = lax.all_gather(packed, "sp").reshape(seq_count, pieces, heads, -1)
    one = everything[..., 2 * value_size :]
    peaks, denominators = (one[..., 0], one[..., 1])
    own_score, gate_new = (one[:, 0, :, 2], one[:, 0, :, 3])
    value_new = everything[:, 0, :, value_size : 2 * value_size]
    top = jnp.maximum(jnp.max(peaks, axis=1), gate_new)
    old = jnp.exp(peaks - top[:, None])
    new = jnp.exp(gate_new - top) * own_score
    total = jnp.sum(old[..., None] * everything[..., :value_size], axis=1)
    total = total + new[..., None] * value_new
    weight = jnp.sum(old * denominators, axis=1) + new
    return total / jnp.maximum(jnp.abs(weight), 1.0)[..., None]


def per_device(
    tokens,
    new_rows,
    new_query,
    norm_gain,
    key_weight,
    value_weight,
    input_weight,
    forget_weight,
    forget_bias,
    gate_offsets,
):
    seq_count, positions, model_width = tokens.shape
    heads = forget_bias.shape[0]
    key_size = key_weight.shape[1] // heads
    group = lax.axis_size("sp")
    shares = lax.axis_size("tp")
    pieces = group // seq_count
    sub = positions // pieces
    rows = group * sub
    index, core = (lax.axis_index("sp"), lax.axis_index("tp"))
    prompt = index // pieces
    part = model_width // shares
    mine = lax.dynamic_slice_in_dim(tokens.reshape(group, sub, model_width), core * part, part, 2)
    moved = lax.all_to_all(mine, "sp", split_axis=0, concat_axis=0, tiled=True)
    source = lax.all_gather(moved.reshape(rows, part), "tp", axis=1, tiled=True)
    offsets = jnp.transpose(gate_offsets.reshape(group, sub, 2 * heads), (0, 2, 1))
    offsets = lax.all_to_all(offsets, "sp", split_axis=0, concat_axis=0, tiled=True)
    offsets = jnp.transpose(offsets, (1, 0, 2)).reshape(2 * heads, rows)
    key_weight = lax.all_gather(key_weight, "sp", axis=0, tiled=True)
    value_weight = lax.all_gather(value_weight, "sp", axis=0, tiled=True)
    normed = normed_rows(source, norm_gain)
    fresh = normed_rows(lax.dynamic_slice_in_dim(new_rows, prompt, 1, 0), norm_gain)
    head_start = core * heads
    gate_weight = jnp.concatenate(
        [
            lax.dynamic_slice_in_dim(input_weight, head_start, heads, 1),
            lax.dynamic_slice_in_dim(forget_weight, head_start, heads, 1),
        ],
        axis=1,
    ).T
    gates = contract_last(gate_weight, normed)
    gate_new = contract_last(gate_weight[:heads], fresh)

    def project(x):
        keys = jnp.dot(x, key_weight, preferred_element_type=jnp.float32) * key_size ** (-0.5)
        values = jnp.dot(x, value_weight, preferred_element_type=jnp.float32)
        return (keys.astype(jnp.bfloat16), values.astype(jnp.bfloat16))

    keys, values = project(normed)
    key_new, value_new = project(fresh)
    log_weight = log_weights(gates, offsets, forget_bias, heads, group, pieces)
    query = lax.dynamic_slice_in_dim(new_query, prompt, 1, 0)
    peak, numerator, denominator = read_part(query, keys, values, log_weight, heads)
    own_score = jnp.sum(
        (query.astype(jnp.float32) * key_new.astype(jnp.float32)).reshape(heads, key_size),
        axis=1,
        keepdims=True,
    )
    value_new = value_new.astype(jnp.float32).reshape(heads, -1)
    read_out = finish(
        peak, numerator, denominator, own_score, gate_new, value_new, seq_count, pieces
    )
    return (
        keys[None],
        values[None],
        log_weight[None],
        read_out.reshape(seq_count, -1).astype(jnp.bfloat16),
    )


def solution(mesh):
    return jax.shard_map(
        per_device,
        mesh=mesh,
        in_specs=(
            P("gr", "sp", None),
            P("gr", None),
            P("gr", "tp"),
            P(),
            P("sp", "tp"),
            P("sp", "tp"),
            P(),
            P(),
            P("tp"),
            P("gr", "sp", None, "tp"),
        ),
        out_specs=(
            P(("gr", "sp"), None, "tp"),
            P(("gr", "sp"), None, "tp"),
            P(("gr", "sp"), "tp", None),
            P("gr", "tp"),
        ),
        check_vma=False,
    )
```

profile of v0, /device:TPU:0, one launch (start us, length us, event | category | flops | bytes accessed | tf_op | source)
XLA Modules:
  0.0 263.4 jit_solution(13032726843708910737)
XLA Ops:
  7.2 0.7 all-gather.8.cloned.1.call-update
  7.9 0.7 all-gather.10.cloned.1.call-update
  8.7 1.8 constant_dynamic-slice_fusion.4
  10.5 80.9 %all_to_all.10 = bf16[8,128,1024]{2,1,0:T(8,128)(2,1)} all-to-all(bf16[8,128,1024]{2,1,0:T(8,128)(2,1)S(1)} %constant_dynamic-slice_fusion.4), channel_id=1, replica_groups=mesh['gr'=2,'sp'=8,'tp'=2] {'sp'}, dimensions={0} | all-to-all | bytes 4194304 | tf_op jit(solution)/shard_map/all_to_all | solution.py:98
  91.5 0.6 copy.36
  92.2 3.6 %all-to-all-start.1 = ((f32[8,16,128]{2,1,0:T(8,128)}), f32[8,16,128]{2,1,0:T(8,128)S(1)}, u32[]{:S(2)}, u32[]{:S(2)}) async-start(f32[8,16,128]{2,1,0:T(8,128)} %copy.36), calls=%async_computation.1 | async-start | bytes 131072 | tf_op jit(solution)/shard_map/all_to_all | solution.py:101
  95.8 0.6 multiply_reduce_fusion
  97.4 2.0 fusion.27
  99.7 61.1 %all-gather.10.cloned.1.call-done = bf16[2048,1024]{1,0:T(8,128)(2,1)} async-done(((bf16[256,1024]{1,0:T(8,128)(2,1)}), bf16[2048,1024]{1,0:T(8,128)(2,1)}) %all-gather.10.cloned.1.call-update) | async-done | bytes 4194320 | tf_op jit(solution)/shard_map/all_gather | solution.py:104
  160.8 2.8 %fusion.29 = f32[1,1024]{1,0:T(1,128)S(1)} fusion(bf16[2048,1024]{1,0:T(8,128)(2,1)} %all-gather.10.cloned.1.call-done, bf16[1,2048]{1,0:T(2,128)(2,1)S(1)} %multiply_multiply_fusion), kind=kOutput, calls=%fused_computation.55 | convolution fusion | flops 4194304 | bytes 4202496 | tf_op jit(solution)/shard_map/dot_general | solution.py:120
  163.6 10.9 %all-gather.6.cloned.1.call-done = bf16[1024,2048]{1,0:T(8,128)(2,1)} async-done(((bf16[1024,1024]{1,0:T(8,128)(2,1)}), bf16[1024,2048]{1,0:T(8,128)(2,1)}) %all-gather.6.cloned.1.call-update) | async-done | bytes 4194320 | tf_op jit(solution)/shard_map/all_gather | solution.py:99
  174.6 3.2 %fusion = f32[1024]{0:T(1024)S(1)} fusion(bf16[1024,2048]{1,0:T(8,128)(2,1)} %all-gather.6.cloned.1.call-done), kind=kLoop, calls=%fused_computation.2 | loop fusion | flops 6290432 | bytes 4198400 | tf_op jit(solution)/shard_map/reduce_sum | solution.py:12
  177.8 0.2 copy-done
  178.0 1.3 fusion.9
  179.3 0.2 fusion.52
  179.5 30.9 %all-gather = f32[64,8]{1,0:T(8,128)S(1)} all-gather(f32[8,8]{1,0:T(8,128)S(1)} %copy.38), channel_id=2, replica_groups=mesh['gr'=2,'sp'=8,'tp'=2] {'sp'}, dimensions={0}, use_global_device_ids=true | all-gather | bytes 2304 | tf_op jit(solution)/shard_map/all_gather | solution.py:30
  210.9 0.3 fusion.4
  211.3 4.6 %multiply_convert_fusion = bf16[1024,512]{1,0:T(8,128)(2,1)S(1)} fusion(bf16[2048,512]{1,0:T(8,128)(2,1)S(1)} %copy-done.1, bf16[1024,2048]{1,0:T(8,128)(2,1)} %all-gather.6.cloned.1.call-done, f32[2048]{0:T(1024)S(1)} %convert_element_type.64, f32[1024]{0:T(1024)S(1)} %add_rsqrt_fusion), kind=kOutput, calls=%fused_computation.5 | convolution fusion | flops 2156920832 | bytes 7352320 | tf_op jit(solution)/shard_map/dot_general | solution.py:119
  215.9 0.5 fusion.54
  216.5 8.0 %convolution_convert_fusion = bf16[1024,1024]{1,0:T(8,128)(2,1)S(1)} fusion(bf16[2048,1024]{1,0:T(8,128)(2,1)} %all-gather.10.cloned.1.call-done, bf16[1024,2048]{1,0:T(8,128)(2,1)} %all-gather.6.cloned.1.call-done, f32[2048]{0:T(1024)S(1)} %convert_element_type.64, f32[1024]{0:T(1024)S(1)} %add_rsqrt_fusion), kind=kOutput, calls=%fused_computation.6 | convolution fusion | flops 4304404480 | bytes 10498048 | tf_op jit(solution)/shard_map/dot_general | solution.py:120
  224.6 0.4 fusion.5
  225.0 30.5 %all-gather.1 = f32[64,384]{1,0:T(8,128)S(1)} all-gather(f32[8,384]{1,0:T(8,128)S(1)} %pad_maximum_fusion.2), channel_id=3, replica_groups=mesh['gr'=2,'sp'=8,'tp'=2] {'sp'}, dimensions={0}, use_global_device_ids=true | all-gather | bytes 110592 | tf_op jit(solution)/shard_map/all_gather | solution.py:60
  255.8 0.2 exponential_reduce_fusion
  256.3 0.6 fusion.24
  (72 shorter events, 2.1 us)
Async XLA Ops:
  7.2 90.2 %all-gather.8.cloned.1.call-start = ((), (), s32[]{:S(2)}) async-start(), calls=%async_computation.3 | async-start | bytes 2359296 | tf_op jit(solution)/shard_map/all_gather | solution.py:103
  7.9 152.9 %all-gather.10.cloned.1.call-start = ((), (), s32[]{:S(2)}) async-start(), calls=%async_computation.4 | async-start | bytes 4718592 | tf_op jit(solution)/shard_map/all_gather | solution.py:104
  8.6 165.9 %all-gather.6.cloned.1.call-start = ((), (), s32[]{:S(2)}) async-start(), calls=%async_computation.2 | async-start | bytes 6291456 | tf_op jit(solution)/shard_map/all_gather | solution.py:99
  10.5 81.0 %copy-start.5 = (f32[4,256,2,8]{1,3,2,0:T(8,128)S(1)}, f32[4,256,2,8]{1,3,2,0:T(8,128)}, u32[]{:S(2)}) copy-start(f32[4,256,2,8]{1,3,2,0:T(8,128)} %param.19) | copy-start | bytes 196612
  10.5 85.3 %copy-start.6 = (bf16[4,2048]{1,0:T(4,128)(2,1)S(1)}, bf16[4,2048]{1,0:T(4,128)(2,1)}, u32[]{:S(2)}) copy-start(bf16[4,2048]{1,0:T(4,128)(2,1)} %param.11) | copy-start | bytes 49156
  10.5 86.6 %copy-start.9 = (bf16[2048]{0:T(1024)(128)(2,1)S(1)}, bf16[2048]{0:T(1024)(128)(2,1)}, u32[]{:S(2)}) copy-start(bf16[2048]{0:T(1024)(128)(2,1)} %param.13) | copy-start | bytes 12292
  10.5 86.6 %copy-start.10 = (bf16[4,512]{1,0:T(4,128)(2,1)S(1)}, bf16[4,512]{1,0:T(4,128)(2,1)}, u32[]{:S(2)}) copy-start(bf16[4,512]{1,0:T(4,128)(2,1)} %param.12) | copy-start | bytes 12292
  10.5 86.7 %copy-start.7 = (bf16[2048,16]{0,1:T(8,128)(2,1)S(1)}, bf16[2048,16]{0,1:T(8,128)(2,1)}, u32[]{:S(2)}) copy-start(bf16[2048,16]{0,1:T(8,128)(2,1)} %param.17) | copy-start | bytes 196612
  10.5 86.7 %copy-start.8 = (bf16[2048,16]{0,1:T(8,128)(2,1)S(1)}, bf16[2048,16]{0,1:T(8,128)(2,1)}, u32[]{:S(2)}) copy-start(bf16[2048,16]{0,1:T(8,128)(2,1)} %param.16) | copy-start | bytes 196612
  92.2 87.1 %all-to-all-start.1 = ((f32[8,16,128]{2,1,0:T(8,128)}), f32[8,16,128]{2,1,0:T(8,128)S(1)}, u32[]{:S(2)}, u32[]{:S(2)}) async-start(f32[8,16,128]{2,1,0:T(8,128)} %copy.36), calls=%async_computation.1 | async-start | bytes 131072 | tf_op jit(solution)/shard_map/all_to_all | solution.py:101
  174.6 3.4 %copy-start = (bf16[1024,2048]{1,0:T(8,128)(2,1)S(1)}, bf16[1024,2048]{1,0:T(8,128)(2,1)}, u32[]{:S(2)}) copy-start(bf16[1024,2048]{1,0:T(8,128)(2,1)} %all-gather.6.cloned.1.call-done) | copy-start | bytes 12582916
  177.8 1.5 copy-start.11
  178.0 33.3 %copy-start.1 = (bf16[2048,512]{1,0:T(8,128)(2,1)S(1)}, bf16[2048,512]{1,0:T(8,128)(2,1)}, u32[]{:S(2)}) copy-start(bf16[2048,512]{1,0:T(8,128)(2,1)} %all-gather.8.cloned.1.call-done) | copy-start | bytes 6291460
  211.3 4.7 %copy-start.4 = (f32[8,1024]{1,0:T(8,128)}, f32[8,1024]{1,0:T(8,128)S(1)}, u32[]{:S(2)}) copy-start(f32[8,1024]{1,0:T(8,128)S(1)} %get-tuple-element.12) | copy-start | bytes 98308
  215.9 8.6 %copy-start.3 = (bf16[1024,512]{1,0:T(8,128)(2,1)}, bf16[1024,512]{1,0:T(8,128)(2,1)S(1)}, u32[]{:S(2)}) copy-start(bf16[1024,512]{1,0:T(8,128)(2,1)S(1)} %multiply_convert_fusion) | copy-start | bytes 3145732
  224.5 32.4 %copy-start.2 = (bf16[1024,1024]{1,0:T(8,128)(2,1)}, bf16[1024,1024]{1,0:T(8,128)(2,1)S(1)}, u32[]{:S(2)}) copy-start(bf16[1024,1024]{1,0:T(8,128)(2,1)S(1)} %convolution_convert_fusion) | copy-start | bytes 6291460
Sparse Core Ops, SparseCore 0:
  10.1 76.4 all-gather.7
  88.7 72.0 all-gather.9
  162.3 12.1 all-gather.5
where the time goes:
time: 264 us; the launch traced here: 263 us
  blocking collectives  142 us (54%)
  waiting for transfers between devices  73.4 us (28%)
  matrix products  19.9 us (8%)
  between operations  14.8 us (6%)
  other arithmetic  5.59 us (2%)
  local copies, waits for them, and re-layouts  3.73 us (1%)
  starting transfers between devices  3.71 us (1%)
    all_to_all x1, blocking collectives, per_device(): moved = lax.all_to_all(mine, 'sp', split_axis=0, concat_axis=0, tiled=True)  80.9 us
    all_gather x1, waiting for transfers between devices, per_device(): value_weight = lax.all_gather(value_weight, 'sp', axis=0, tiled=True)  61.1 us
    all_gather x1, blocking collectives, log_weights(): everything = lax.all_gather(totals, 'sp')  30.9 us
    all_gather x1, blocking collectives, finish(): lax.all_gather(packed, 'sp').reshape(seq_count, pieces, heads, -1)  30.5 us
    all_gather x1, waiting for transfers between devices, per_device(): source = lax.all_gather(moved.reshape(rows, part), 'tp', axis=1, tiled=True)  10.9 us
    dot_general x2, matrix products, project(): values = jnp.dot(x, value_weight, preferred_element_type=jnp.float32)  10.8 us
    dot_general x2, matrix products, project(): jnp.dot(x, key_weight, preferred_element_type=jnp.float32)  6.53 us
  transfers between devices with their start and end apart: 4, of which 2 were waited for; matrix products, arithmetic and copies ran while one was open for 5% of the time, Pallas kernels for 0%

commit v1 on v0

--- a/solution.py
+++ b/solution.py
@@ -101,7 +101,22 @@
     offsets = lax.all_to_all(offsets, "sp", split_axis=0, concat_axis=0, tiled=True)
     offsets = jnp.transpose(offsets, (1, 0, 2)).reshape(2 * heads, rows)
     key_weight = lax.all_gather(key_weight, "sp", axis=0, tiled=True)
-    value_weight = lax.all_gather(value_weight, "sp", axis=0, tiled=True)
+    k_all = jax.lax.axis_size("sp")
+    nodes = []
+    u = 1
+    while u < k_all:
+        nodes.append((u - 1, u))
+        u += 1
+    base_arr = nodes + [(k_all - 1, 0)]
+    then = value_weight
+    grid = [then]
+    num = 0
+    while num < k_all - 1:
+        then = jax.lax.ppermute(then, perm=base_arr, axis_name="sp")
+        grid += [then]
+        num = num + 1
+    value_now = jnp.concatenate([*reversed(grid)], axis=0)
+    value_weight = jnp.roll(value_now, (jax.lax.axis_index("sp") + 1) * then.shape[0], axis=0)
     normed = normed_rows(source, norm_gain)
     fresh = normed_rows(lax.dynamic_slice_in_dim(new_rows, prompt, 1, 0), norm_gain)
     head_start = core * heads

time: 264 us -> 287 us (1.087)
  blocking collectives: 142 us -> 61.1 us
  waiting for transfers between devices: 73.4 us -> 139 us
  starting transfers between devices: 3.71 us -> 30.7 us
  local copies, waits for them, and re-layouts: 3.73 us -> 14.7 us
    ppermute x0 -> x7, waiting for transfers between devices: none -> 138 us  [per_device(): then = jax.lax.ppermute(then, perm=base_arr, axis_name='sp')]
    all_to_all x1 -> x0, blocking collectives: 80.9 us -> none  [per_device(): moved = lax.all_to_all(mine, 'sp', split_axis=0, concat_axis=0, tiled=True)]
    all_gather x1 -> x0, waiting for transfers between devices: 61.1 us -> none  [per_device(): value_weight = lax.all_gather(value_weight, 'sp', axis=0, tiled=True)]
    all_gather x1, waiting for transfers between devices: 10.9 us -> 0.01 us  [per_device(): source = lax.all_gather(moved.reshape(rows, part), 'tp', axis=1, tiled=True)]
    all_to_all x1, starting transfers between devices: 3.59 us -> 13.6 us  [per_device(): lax.all_to_all(offsets, 'sp', split_axis=0, concat_axis=0, tiled=True)]
    ppermute x0 -> x7, starting transfers between devices: none -> 9.76 us  [per_device(): then = jax.lax.ppermute(then, perm=base_arr, axis_name='sp')]
    unnamed x30 -> x53, local copies, waits for them, and re-layouts: 0.6 us -> 10.2 us
    all_to_all x0 -> x1, starting transfers between devices: none -> 7.31 us  [per_device(): moved = lax.all_to_all(mine, 'sp', split_axis=0, concat_axis=0, tiled=True)]
  transfers between devices with their start and end apart: 4 -> 11, of which waited for: 2 -> 6; matrix products, arithmetic and copies ran while one was open for 5% -> 6% of each run, Pallas kernels for 0% -> 0%
where the time goes in v1:
time: 287 us
  waiting for transfers between devices  139 us (48%)
  blocking collectives  61.1 us (21%)
  starting transfers between devices  30.7 us (11%)
  matrix products  19.9 us (7%)
  between operations  15.2 us (5%)
  local copies, waits for them, and re-layouts  14.7 us (5%)
  other arithmetic  5.44 us (2%)
    ppermute x7, waiting for transfers between devices, per_device(): then = jax.lax.ppermute(then, perm=base_arr, axis_name='sp')  138 us
    all_gather x1, blocking collectives, log_weights(): everything = lax.all_gather(totals, 'sp')  30.6 us
    all_gather x1, blocking collectives, finish(): lax.all_gather(packed, 'sp').reshape(seq_count, pieces, heads, -1)  30.5 us
    all_to_all x1, starting transfers between devices, per_device(): lax.all_to_all(offsets, 'sp', split_axis=0, concat_axis=0, tiled=True)  13.6 us
    unnamed x53, local copies, waits for them, and re-layouts  10.2 us
    ppermute x7, starting transfers between devices, per_device(): then = jax.lax.ppermute(then, perm=base_arr, axis_name='sp')  9.76 us
    dot_general x2, matrix products, project(): values = jnp.dot(x, value_weight, preferred_element_type=jnp.float32)  8.65 us
    all_to_all x1, starting transfers between devices, per_device(): moved = lax.all_to_all(mine, 'sp', split_axis=0, concat_axis=0, tiled=True)  7.31 us
  transfers between devices with their start and end apart: 11, of which 6 were waited for; matrix products, arithmetic and copies ran while one was open for 6% of the time, Pallas kernels for 0%

profile of v1, /device:TPU:0, one launch (start us, length us, event | category | flops | bytes accessed | tf_op | source)
XLA Modules:
  0.0 286.6 jit_solution(12414046209437848840)
XLA Ops:
  7.2 3.1 %constant_dynamic-slice_fusion.4 = bf16[8,128,1024]{2,1,0:T(8,128)(2,1)} fusion(bf16[8,128,2048]{2,1,0:T(8,128)(2,1)} %bitcast.98, s32[]{:T(128)S(6)} %select_n.61), kind=kLoop, calls=%fused_computation.115 | loop fusion | bytes 4194308 | tf_op jit(solution)/shard_map/dynamic_slice | solution.py:97
  10.4 7.3 %all-to-all-start = ((bf16[8,128,1024]{2,1,0:T(8,128)(2,1)}), bf16[8,128,1024]{2,1,0:T(8,128)(2,1)S(1)}, u32[]{:S(2)}, u32[]{:S(2)}) async-start(bf16[8,128,1024]{2,1,0:T(8,128)(2,1)} %constant_dynamic-slice_fusion.4), calls=%async_computation | async-start | bytes 4194304 | tf_op jit(solution)/shard_map/all_to_all | solution.py:98
  18.4 2.1 collective-permute-start
  20.5 61.0 %collective-permute-done = bf16[256,1024]{1,0:T(8,128)(2,1)S(1)} collective-permute-done((bf16[256,1024]{1,0:T(8,128)(2,1)S(1)}, bf16[256,1024]{1,0:T(8,128)(2,1)S(1)}, u32[]{:S(2)}, u32[]{:S(2)}) %collective-permute-start) | collective-permute-done | bytes 524320 | tf_op jit(solution)/shard_map/ppermute | solution.py:115
  81.5 22.7 %collective-permute-done.1 = bf16[256,1024]{1,0:T(8,128)(2,1)S(1)} collective-permute-done((bf16[256,1024]{1,0:T(8,128)(2,1)S(1)}, bf16[256,1024]{1,0:T(8,128)(2,1)S(1)}, u32[]{:S(2)}, u32[]{:S(2)}) %collective-permute-start.1) | collective-permute-done | bytes 524320 | tf_op jit(solution)/shard_map/ppermute | solution.py:115
  105.1 13.9 %collective-permute-done.2 = bf16[256,1024]{1,0:T(8,128)(2,1)} collective-permute-done((bf16[256,1024]{1,0:T(8,128)(2,1)S(1)}, bf16[256,1024]{1,0:T(8,128)(2,1)}, u32[]{:S(2)}, u32[]{:S(2)}) %collective-permute-start.2) | collective-permute-done | bytes 524320 | tf_op jit(solution)/shard_map/ppermute | solution.py:115
  119.0 5.6 %collective-permute-start.3 = (bf16[256,1024]{1,0:T(8,128)(2,1)}, bf16[256,1024]{1,0:T(8,128)(2,1)}, u32[]{:S(2)}, u32[]{:S(2)}) collective-permute-start(bf16[256,1024]{1,0:T(8,128)(2,1)} %collective-permute-done.2), channel_id=1, source_target_pairs={{0,2},{2,4},{4,6},{6,8},{8,10},{10,12},{12,14},{14,0},{1,3},{3,5},... | collective-permute-start | bytes 1572872 | tf_op jit(solution)/shard_map/ppermute | solution.py:115
  125.4 13.6 %all-to-all-start.1 = ((f32[8,16,128]{2,1,0:T(8,128)}), f32[8,16,128]{2,1,0:T(8,128)S(1)}, u32[]{:S(2)}, u32[]{:S(2)}) async-start(f32[8,16,128]{2,1,0:T(8,128)} %copy.36), calls=%async_computation.1 | async-start | bytes 131072 | tf_op jit(solution)/shard_map/all_to_all | solution.py:101
  141.1 2.1 collective-permute-start.4
  143.3 13.9 %collective-permute-done.4 = bf16[256,1024]{1,0:T(8,128)(2,1)S(1)} collective-permute-done((bf16[256,1024]{1,0:T(8,128)(2,1)}, bf16[256,1024]{1,0:T(8,128)(2,1)S(1)}, u32[]{:S(2)}, u32[]{:S(2)}) %collective-permute-start.4) | collective-permute-done | bytes 524320 | tf_op jit(solution)/shard_map/ppermute | solution.py:115
  157.3 14.8 %collective-permute-done.5 = bf16[256,1024]{1,0:T(8,128)(2,1)S(1)} collective-permute-done((bf16[256,1024]{1,0:T(8,128)(2,1)S(1)}, bf16[256,1024]{1,0:T(8,128)(2,1)S(1)}, u32[]{:S(2)}, u32[]{:S(2)}) %collective-permute-start.5) | collective-permute-done | bytes 524320 | tf_op jit(solution)/shard_map/ppermute | solution.py:115
  172.1 2.0 fusion.34
  174.3 11.8 %collective-permute-done.6 = bf16[256,1024]{1,0:T(8,128)(2,1)S(1)} collective-permute-done((bf16[256,1024]{1,0:T(8,128)(2,1)S(1)}, bf16[256,1024]{1,0:T(8,128)(2,1)S(1)}, u32[]{:S(2)}, u32[]{:S(2)}) %collective-permute-start.6) | collective-permute-done | bytes 524320 | tf_op jit(solution)/shard_map/ppermute | solution.py:115
  186.2 1.1 constant_dynamic-update-slice_fusion.12
  187.3 1.1 constant_dynamic-update-slice_fusion.11
  188.4 1.1 constant_dynamic-update-slice_fusion.10
  189.7 1.1 constant_dynamic-update-slice_fusion.4
  192.0 3.2 %copy-done.1 = bf16[4096,1024]{1,0:T(8,128)(2,1)} copy-done((bf16[4096,1024]{1,0:T(8,128)(2,1)}, bf16[4096,1024]{1,0:T(8,128)(2,1)S(1)}, u32[]{:S(2)}) %copy-start.1) | copy-done | bytes 8388632
  195.9 3.1 %fusion = f32[1024]{0:T(1024)S(1)} fusion(bf16[1024,2048]{1,0:T(8,128)(2,1)} %all-gather.5.cloned.1.call-done), kind=kLoop, calls=%fused_computation.2 | loop fusion | flops 6290432 | bytes 4198400 | tf_op jit(solution)/shard_map/reduce_sum | solution.py:12
  199.0 3.4 %fusion.16 = f32[16,1024]{1,0:T(8,128)S(1)} fusion(bf16[2048,8]{0,1:T(8,128)(2,1)S(1)} %get-tuple-element.19, bf16[2048,8]{0,1:T(8,128)(2,1)S(1)} %get-tuple-element.20, bf16[1024,2048]{1,0:T(8,128)(2,1)} %all-gather.5.cloned.1.call-done, f32[2048]{0:T(1024)S(1)} %convert_element_type.64, f32[1024]{0:T(1024)S(1)} %add_rsqrt_fusion), kind=kOutput, calls=%fused_computation.24 | convolution fusion | flops 75628544 | bytes 4337664 | tf_op jit(solution)/shard_map/dot_general | solution.py:17
  202.7 30.6 %all-gather = f32[64,8]{1,0:T(8,128)S(1)} all-gather(f32[8,8]{1,0:T(8,128)S(1)} %copy.38), channel_id=2, replica_groups=mesh['gr'=2,'sp'=8,'tp'=2] {'sp'}, dimensions={0}, use_global_device_ids=true | all-gather | bytes 2304 | tf_op jit(solution)/shard_map/all_gather | solution.py:30
  234.1 4.6 %multiply_convert_fusion = bf16[1024,512]{1,0:T(8,128)(2,1)S(1)} fusion(bf16[2048,512]{1,0:T(8,128)(2,1)S(1)} %copy-done.2, bf16[1024,2048]{1,0:T(8,128)(2,1)} %all-gather.5.cloned.1.call-done, f32[2048]{0:T(1024)S(1)} %convert_element_type.64, f32[1024]{0:T(1024)S(1)} %add_rsqrt_fusion), kind=kOutput, calls=%fused_computation.9 | convolution fusion | flops 2156920832 | bytes 7352320 | tf_op jit(solution)/shard_map/dot_general | solution.py:134
  239.3 8.0 %fusion.7 = bf16[1024,1024]{1,0:T(8,128)(2,1)S(1)} fusion(bf16[4096,1024]{1,0:T(8,128)(2,1)} %copy-done.1, s32[]{:T(128)S(6)} %select_n.63, bf16[1024,2048]{1,0:T(8,128)(2,1)} %all-gather.5.cloned.1.call-done, f32[2048]{0:T(1024)S(1)} %convert_element_type.64, f32[1024]{0:T(1024)S(1)} %add_rsqrt_fusion), kind=kOutput, calls=%fused_computation.10 | convolution fusion | flops 4304404480 | bytes 10498052 | tf_op jit(solution)/shard_map/dot_general | solution.py:135
  247.8 30.5 %all-gather.1 = f32[64,384]{1,0:T(8,128)S(1)} all-gather(f32[8,384]{1,0:T(8,128)S(1)} %pad_maximum_fusion.2), channel_id=3, replica_groups=mesh['gr'=2,'sp'=8,'tp'=2] {'sp'}, dimensions={0}, use_global_device_ids=true | all-gather | bytes 110592 | tf_op jit(solution)/shard_map/all_gather | solution.py:60
  (108 shorter events, 9.7 us)
Async XLA Ops:
  7.2 11.3 %copy-start.4 = (bf16[256,1024]{1,0:T(8,128)(2,1)S(1)}, bf16[256,1024]{1,0:T(8,128)(2,1)}, u32[]{:S(2)}) copy-start(bf16[256,1024]{1,0:T(8,128)(2,1)} %param.15) | copy-start | bytes 1572868
  7.2 117.4 %copy-start.9 = (f32[4,256,2,8]{1,3,2,0:T(8,128)S(1)}, f32[4,256,2,8]{1,3,2,0:T(8,128)}, u32[]{:S(2)}) copy-start(f32[4,256,2,8]{1,3,2,0:T(8,128)} %param.19) | copy-start | bytes 196612
  7.2 118.1 %copy-start.12 = (bf16[2048,16]{0,1:T(8,128)(2,1)S(1)}, bf16[2048,16]{0,1:T(8,128)(2,1)}, u32[]{:S(2)}) copy-start(bf16[2048,16]{0,1:T(8,128)(2,1)} %param.16) | copy-start | bytes 196612
  7.2 118.1 %copy-start.11 = (bf16[2048,16]{0,1:T(8,128)(2,1)S(1)}, bf16[2048,16]{0,1:T(8,128)(2,1)}, u32[]{:S(2)}) copy-start(bf16[2048,16]{0,1:T(8,128)(2,1)} %param.17) | copy-start | bytes 196612
  7.2 132.5 %copy-start.13 = (bf16[2048]{0:T(1024)(128)(2,1)S(1)}, bf16[2048]{0:T(1024)(128)(2,1)}, u32[]{:S(2)}) copy-start(bf16[2048]{0:T(1024)(128)(2,1)} %param.13) | copy-start | bytes 12292
  7.2 132.5 %copy-start.10 = (bf16[4,2048]{1,0:T(4,128)(2,1)S(1)}, bf16[4,2048]{1,0:T(4,128)(2,1)}, u32[]{:S(2)}) copy-start(bf16[4,2048]{1,0:T(4,128)(2,1)} %param.11) | copy-start | bytes 49156
  7.2 133.9 %copy-start.14 = (bf16[4,512]{1,0:T(4,128)(2,1)S(1)}, bf16[4,512]{1,0:T(4,128)(2,1)}, u32[]{:S(2)}) copy-start(bf16[4,512]{1,0:T(4,128)(2,1)} %param.12) | copy-start | bytes 12292
  10.4 115.0 %all-to-all-start = ((bf16[8,128,1024]{2,1,0:T(8,128)(2,1)}), bf16[8,128,1024]{2,1,0:T(8,128)(2,1)S(1)}, u32[]{:S(2)}, u32[]{:S(2)}) async-start(bf16[8,128,1024]{2,1,0:T(8,128)(2,1)} %constant_dynamic-slice_fusion.4), calls=%async_computation | async-start | bytes 4194304 | tf_op jit(solution)/shard_map/all_to_all | solution.py:98
  17.7 154.4 %all-gather.7.cloned.1.call-start = ((), (), s32[]{:S(2)}) async-start(), calls=%async_computation.3 | async-start | bytes 2359296 | tf_op jit(solution)/shard_map/all_gather | solution.py:103
  18.4 63.1 %collective-permute-start = (bf16[256,1024]{1,0:T(8,128)(2,1)S(1)}, bf16[256,1024]{1,0:T(8,128)(2,1)S(1)}, u32[]{:S(2)}, u32[]{:S(2)}) collective-permute-start(bf16[256,1024]{1,0:T(8,128)(2,1)S(1)} %copy-done.4), channel_id=1, source_target_pairs={{0,2},{2,4},{4,6},{6,8},{8,10},{10,12},{12,14},{14,0},{1,3},{3,5},... | collective-permute-start | bytes 1572872 | tf_op jit(solution)/shard_map/ppermute | solution.py:115
  81.5 22.7 %collective-permute-start.1 = (bf16[256,1024]{1,0:T(8,128)(2,1)S(1)}, bf16[256,1024]{1,0:T(8,128)(2,1)S(1)}, u32[]{:S(2)}, u32[]{:S(2)}) collective-permute-start(bf16[256,1024]{1,0:T(8,128)(2,1)S(1)} %collective-permute-done), channel_id=1, source_target_pairs={{0,2},{2,4},{4,6},{6,8},{8,10},{10,12},{12,14},{14,0},{1,3},{3,5},... | collective-permute-start | bytes 1572872 | tf_op jit(solution)/shard_map/ppermute | solution.py:115
  105.0 13.9 %collective-permute-start.2 = (bf16[256,1024]{1,0:T(8,128)(2,1)S(1)}, bf16[256,1024]{1,0:T(8,128)(2,1)}, u32[]{:S(2)}, u32[]{:S(2)}) collective-permute-start(bf16[256,1024]{1,0:T(8,128)(2,1)S(1)} %collective-permute-done.1), channel_id=1, source_target_pairs={{0,2},{2,4},{4,6},{6,8},{8,10},{10,12},{12,14},{14,0},{1,3},{3,5},... | collective-permute-start | bytes 1572872 | tf_op jit(solution)/shard_map/ppermute | solution.py:115
  119.0 22.1 %collective-permute-start.3 = (bf16[256,1024]{1,0:T(8,128)(2,1)}, bf16[256,1024]{1,0:T(8,128)(2,1)}, u32[]{:S(2)}, u32[]{:S(2)}) collective-permute-start(bf16[256,1024]{1,0:T(8,128)(2,1)} %collective-permute-done.2), channel_id=1, source_target_pairs={{0,2},{2,4},{4,6},{6,8},{8,10},{10,12},{12,14},{14,0},{1,3},{3,5},... | collective-permute-start | bytes 1572872 | tf_op jit(solution)/shard_map/ppermute | solution.py:115
  125.4 13.6 %copy-start = (bf16[8,128,1024]{2,1,0:T(8,128)(2,1)}, bf16[8,128,1024]{2,1,0:T(8,128)(2,1)S(1)}, u32[]{:S(2)}) copy-start(bf16[8,128,1024]{2,1,0:T(8,128)(2,1)S(1)} %all-to-all-done) | copy-start | bytes 6291460
  125.4 77.1 %all-to-all-start.1 = ((f32[8,16,128]{2,1,0:T(8,128)}), f32[8,16,128]{2,1,0:T(8,128)S(1)}, u32[]{:S(2)}, u32[]{:S(2)}) async-start(f32[8,16,128]{2,1,0:T(8,128)} %copy.36), calls=%async_computation.1 | async-start | bytes 131072 | tf_op jit(solution)/shard_map/all_to_all | solution.py:101
  138.9 57.0 %all-gather.5.cloned.1.call-start = ((), (), s32[]{:S(2)}) async-start(), calls=%async_computation.2 | async-start | bytes 6291456 | tf_op jit(solution)/shard_map/all_gather | solution.py:99
  139.7 52.2 %copy-start.6 = (bf16[256,1024]{1,0:T(8,128)(2,1)S(1)}, bf16[256,1024]{1,0:T(8,128)(2,1)}, u32[]{:S(2)}) copy-start(bf16[256,1024]{1,0:T(8,128)(2,1)} %copy-done.5) | copy-start | bytes 1572868
  141.1 16.0 %collective-permute-start.4 = (bf16[256,1024]{1,0:T(8,128)(2,1)}, bf16[256,1024]{1,0:T(8,128)(2,1)S(1)}, u32[]{:S(2)}, u32[]{:S(2)}) collective-permute-start(bf16[256,1024]{1,0:T(8,128)(2,1)} %collective-permute-done.3), channel_id=1, source_target_pairs={{0,2},{2,4},{4,6},{6,8},{8,10},{10,12},{12,14},{14,0},{1,3},{3,5},... | collective-permute-start | bytes 1572872 | tf_op jit(solution)/shard_map/ppermute | solution.py:115
  157.2 14.9 %collective-permute-start.5 = (bf16[256,1024]{1,0:T(8,128)(2,1)S(1)}, bf16[256,1024]{1,0:T(8,128)(2,1)S(1)}, u32[]{:S(2)}, u32[]{:S(2)}) collective-permute-start(bf16[256,1024]{1,0:T(8,128)(2,1)S(1)} %collective-permute-done.4), channel_id=1, source_target_pairs={{0,2},{2,4},{4,6},{6,8},{8,10},{10,12},{12,14},{14,0},{1,3},{3,5},... | collective-permute-start | bytes 1572872 | tf_op jit(solution)/shard_map/ppermute | solution.py:115
  172.1 14.0 %collective-permute-start.6 = (bf16[256,1024]{1,0:T(8,128)(2,1)S(1)}, bf16[256,1024]{1,0:T(8,128)(2,1)S(1)}, u32[]{:S(2)}, u32[]{:S(2)}) collective-permute-start(bf16[256,1024]{1,0:T(8,128)(2,1)S(1)} %collective-permute-done.5), channel_id=1, source_target_pairs={{0,2},{2,4},{4,6},{6,8},{8,10},{10,12},{12,14},{14,0},{1,3},{3,5},... | collective-permute-start | bytes 1572872 | tf_op jit(solution)/shard_map/ppermute | solution.py:115
  195.2 7.2 %copy-start.15 = (f32[8]{0:T(128)S(1)}, f32[8]{0:T(128)}, u32[]{:S(2)}) copy-start(f32[8]{0:T(128)} %param.18) | copy-start | bytes 100
  195.2 38.8 %copy-start.2 = (bf16[2048,512]{1,0:T(8,128)(2,1)S(1)}, bf16[2048,512]{1,0:T(8,128)(2,1)}, u32[]{:S(2)}) copy-start(bf16[2048,512]{1,0:T(8,128)(2,1)} %all-gather.7.cloned.1.call-done) | copy-start | bytes 6291460
  238.7 8.7 %copy-start.7 = (bf16[1024,512]{1,0:T(8,128)(2,1)}, bf16[1024,512]{1,0:T(8,128)(2,1)S(1)}, u32[]{:S(2)}) copy-start(bf16[1024,512]{1,0:T(8,128)(2,1)S(1)} %multiply_convert_fusion) | copy-start | bytes 3145732
  247.4 32.4 %copy-start.3 = (bf16[1024,1024]{1,0:T(8,128)(2,1)}, bf16[1024,1024]{1,0:T(8,128)(2,1)S(1)}, u32[]{:S(2)}) copy-start(bf16[1024,1024]{1,0:T(8,128)(2,1)S(1)} %fusion.7) | copy-start | bytes 6291460
  (3 other events, 9.1 us)
Sparse Core Ops, SparseCore 0:
  20.6 85.1 all-gather.6
  141.9 15.0 all-gather.4
